TPU v7x, 256 devices: a whole 4x4x8 slice. The times are simulated.
256 devices in a mesh: sp: 32 (over z, y), tp: 8 (over x, core).
Axes of the slice: x: 4, y: 4, z: 8, core: 2. Of those that a mesh axis runs over, the one named last changes fastest.
Arguments:
- tokens: bfloat16 [32768, 4096], P('sp', 'tp'), may hold values from -6 to 6
- norm_gain: float32 [4096], replicated, may hold values from 0.1 to 1.9
- pool_in_weight: bfloat16 [4096, 2048], P('sp', 'tp'), may hold values from -0.09375 to 0.09375
- query_weight: bfloat16 [4096, 2048], P('sp', 'tp'), may hold values from -1 to 1, as said below
- key_weight: bfloat16 [4096, 512], P('sp', 'tp'), may hold values from -40 to 40
- value_weight: bfloat16 [4096, 512], P('sp', 'tp'), may hold values from -0.09375 to 0.09375
- pool_weight: bfloat16 [8, 256, 256], P('tp'), may hold values from -0.375 to 0.375
- pool_scale: float32 [2048], P('tp'), may hold values from 0.1 to 1.9
- sink_logit: float32 [32], P('tp'), may hold values from 3 to 7
- out_pool_weight: bfloat16 [2048, 4096], P('tp', 'sp'), may hold values from -0.09375 to 0.09375
- out_attn_weight: bfloat16 [2048, 4096], P('tp', 'sp'), may hold values from -1.5 to 1.5
Outputs:
- mixed: bfloat16 [32768, 4096], P(('sp', 'tp'))
Inputs may be any that keep to these rules, and one draw needn't show every extreme that they name: `query_weight`: entries of order 4096 ** -0.5, drawn independently.
All inputs are finite; a program needn't handle non-finite values.
Results may differ from a plain program's by a relative error of at most 0.014.
The roundings to bfloat16 on the way count: a program that leaves them out, or rounds other values in their place, can miss the bound.
Values may be sent and summed in bfloat16 or wider, within the bound.
No kernel may reach another device: no remote copies, remote signals or barrier semaphores. Data moves between devices by JAX's collectives and lax.ppermute only.
A program may use at most 128 MiB of HBM per device.

v0:
```python
import jax
import jax.numpy as jnp
from jax import lax
from jax.sharding import Mesh
from jax.sharding import PartitionSpec as P

HEAD_DIM = 64
Q_HEADS = 32
KV_HEADS = 8
GROUP_DIM = 256
WINDOW = 128
GRID_W = 64
SP = ("sp_0", "sp_1")
SP_TP = ("sp_0", "sp_1", "tp")
epsilon = 1e-06
rotary_base = 10000.0
masked_score = -1e30


def sent_together(arrays, axis, dim, along):
    widths = [a.shape[along] for a in arrays]
    both = jnp.concatenate(arrays, axis=along)
    result = lax.all_gather(both, axis, axis=dim, tiled=True)
    return tuple(jnp.split(result, [sum(widths[:k]) for k in range(1, len(widths))], axis=along))


def padded_2(block, sides, width):
    for axis, dim in sides:
        count = lax.axis_size(axis)
        forward = [(i, i + 1) for i in range(count - 1)]
        backward = [(target, source) for source, target in forward]
        low = lax.ppermute(
            lax.slice_in_dim(block, block.shape[dim] - width, None, axis=dim), axis, forward
        )
        high = lax.ppermute(lax.slice_in_dim(block, 0, width, axis=dim), axis, backward)
        block = jnp.concatenate([low, block, high], axis=dim)
    return block


def gather_axes(array, axes, dim):
    if not axes:
        return array
    nearer = lax.all_gather(array, axes[-1], axis=dim, tiled=True)
    return gather_axes(nearer, axes[:-1], dim)


def rms_normed(values, gain):
    floats = values.astype(jnp.float32)
    scaled = floats * lax.rsqrt(jnp.mean(floats * floats, axis=-1, keepdims=True) + epsilon)
    return (scaled * gain).astype(jnp.bfloat16)


def rotary_tables(positions, head_dim, grid_width):
    freq_count = head_dim // 4
    inverse = rotary_base ** (-jnp.arange(freq_count, dtype=jnp.float32) / freq_count)
    row_pos = (positions // grid_width).astype(jnp.float32)
    col_pos = (positions % grid_width).astype(jnp.float32)
    angles = jnp.stack([row_pos[:, None] * inverse, col_pos[:, None] * inverse], axis=1)
    return (jnp.cos(angles), jnp.sin(angles))


def rotate(values, cosine, sine):
    length, heads, head_dim = values.shape
    split = values.reshape(length, heads, 2, 2, head_dim // 4)
    first = split[:, :, :, 0]
    second = split[:, :, :, 1]
    cos_b = cosine[:, None]
    sin_b = sine[:, None]
    turned = jnp.stack([first * cos_b - second * sin_b, second * cos_b + first * sin_b], axis=3)
    return turned.reshape(length, heads, head_dim)


def shards(
    tokens,
    norm_gain,
    pool_in_weight,
    query_weight,
    key_weight,
    value_weight,
    pool_weight,
    pool_scale,
    sink_logit,
    out_pool_weight,
    out_attn_weight,
):
    whole_rows = lax.all_gather(tokens, "tp", axis=1, tiled=True)
    normed = rms_normed(whole_rows, norm_gain)
    tok_rows = normed.shape[0]

    def project(piece):
        return jnp.dot(normed, piece, preferred_element_type=jnp.float32)

    pieces = sent_together((pool_in_weight, query_weight, key_weight, value_weight), SP, 0, 1)
    pool_raw, query_raw, key_raw, value_raw = tuple((project(piece) for piece in pieces))
    sp_index = lax.axis_index(SP)
    tp_index = lax.axis_index("tp")
    total_rows = tok_rows * lax.axis_size(SP)
    offset = sp_index * tok_rows
    positions = offset + jnp.arange(tok_rows, dtype=jnp.int32)
    cosine, sine = rotary_tables(positions, HEAD_DIM, GRID_W)
    pool_in = pool_raw.astype(jnp.bfloat16)
    queries = rotate(query_raw.reshape(tok_rows, -1, HEAD_DIM), cosine, sine).astype(jnp.bfloat16)
    key_part = rotate(key_raw.reshape(tok_rows, -1, HEAD_DIM), cosine, sine).astype(jnp.bfloat16)
    key_part = key_part.reshape(tok_rows, -1)
    value_part = value_raw.astype(jnp.bfloat16)
    kv_rows = jnp.concatenate([key_part, value_part], axis=1)
    kv_width = key_part.shape[1]
    channels = pool_in.shape[1]
    pool_reach = 8
    rim_depth = max(WINDOW, pool_reach)
    padded = padded_2(jnp.concatenate([pool_in, kv_rows], axis=1), ((SP, 0),), rim_depth)
    pool_pad = padded[rim_depth - pool_reach : rim_depth + tok_rows + pool_reach, :channels]
    kv_pad = padded[rim_depth - WINDOW : rim_depth + tok_rows + WINDOW, channels:]
    running = jnp.concatenate(
        [jnp.zeros((1, channels), jnp.float32), jnp.cumsum(pool_pad.astype(jnp.float32), axis=0)],
        axis=0,
    )
    groups_dev = channels // GROUP_DIM
    selector = (tp_index * groups_dev + jnp.arange(channels, dtype=jnp.int32) // GROUP_DIM) % 4
    window_mean = jnp.zeros((tok_rows, channels), jnp.float32)
    for level, half_width in enumerate((1, 2, 4, 8)):
        window_sum = (
            running[pool_reach + half_width : pool_reach + half_width + tok_rows]
            - running[pool_reach - half_width : pool_reach - half_width + tok_rows]
        )
        counts = jnp.minimum(positions + half_width, total_rows) - jnp.maximum(
            positions - half_width, 0
        )
        level_mean = window_sum / counts.astype(jnp.float32)[:, None]
        window_mean = jnp.where((selector == level)[None, :], level_mean, window_mean)
    pooled = (window_mean - pool_in.astype(jnp.float32)).astype(jnp.bfloat16)
    mixing = jnp.einsum(
        "tgc,gcd->tgd",
        pooled.reshape(tok_rows, groups_dev, GROUP_DIM),
        pool_weight,
        preferred_element_type=jnp.float32,
    )
    pool_out = (mixing.reshape(tok_rows, channels) * pool_scale).astype(jnp.bfloat16)
    group = Q_HEADS // KV_HEADS
    kv_heads_dev = kv_width // HEAD_DIM
    query_groups = queries.reshape(tok_rows, kv_heads_dev, group, HEAD_DIM)
    key_pad = kv_pad[:, :kv_width].reshape(-1, kv_heads_dev, HEAD_DIM)
    value_pad = kv_pad[:, kv_width:].reshape(-1, kv_heads_dev, HEAD_DIM)
    scores = jnp.einsum(
        "qkgd,skd->kgqs", query_groups, key_pad, preferred_element_type=jnp.float32
    ) * HEAD_DIM ** (-0.5)
    key_pos = offset - WINDOW + jnp.arange(tok_rows + 2 * WINDOW, dtype=jnp.int32)
    allowed = (
        (jnp.abs(key_pos[None, :] - positions[:, None]) <= WINDOW)
        & (key_pos >= 0)[None, :]
        & (key_pos < total_rows)[None, :]
    )
    scores = jnp.where(allowed, scores, masked_score)
    sink = sink_logit.reshape(kv_heads_dev, group, 1, 1)
    highest = jnp.maximum(jnp.max(scores, axis=-1, keepdims=True), sink)
    expo = jnp.exp(scores - highest)
    denominator = jnp.sum(expo, axis=-1, keepdims=True) + jnp.exp(sink - highest)
    weights = (expo / denominator).astype(jnp.bfloat16)
    attended = jnp.einsum("kgqs,skd->qkgd", weights, value_pad, preferred_element_type=jnp.float32)
    attn_out = attended.reshape(tok_rows, -1).astype(jnp.bfloat16)
    out_pool_full, out_attn_full = (
        gather_axes(out_pool_weight, SP, 1),
        gather_axes(out_attn_weight, SP, 1),
    )
    return lax.psum_scatter(
        (
            jnp.dot(pool_out, out_pool_full, preferred_element_type=jnp.float32)
            + jnp.dot(attn_out, out_attn_full, preferred_element_type=jnp.float32)
        ).astype(jnp.bfloat16),
        "tp",
        scatter_dimension=0,
        tiled=True,
    )


def solution(mesh):
    finer = Mesh(mesh.devices.reshape(8, 4, mesh.shape["tp"]), ("sp_0", "sp_1", "tp"))
    return jax.shard_map(
        shards,
        mesh=finer,
        in_specs=(
            P(SP, "tp"),
            P(),
            P(SP, "tp"),
            P(SP, "tp"),
            P(SP, "tp"),
            P(SP, "tp"),
            P("tp", None, None),
            P("tp"),
            P("tp"),
            P("tp", SP),
            P("tp", SP),
        ),
        out_specs=P(SP_TP, None),
        check_vma=False,
    )
```

profile of v0, /device:TPU:1, one launch (start us, length us, event | category | flops | bytes accessed | tf_op | source)
XLA Modules:
  0.0 306.1 jit_solution(10103627928105953874)
XLA Ops:
  6.5 0.0 copy-start
  6.5 0.0 all-gather.5.cloned.1.call-start
  6.5 0.7 all-gather.5.cloned.1.call-update
  7.3 0.0 all-gather.7.cloned.1.call-start
  7.3 0.8 copy.17
  8.1 0.8 copy.18
  9.0 1.6 pad_maximum_fusion.2
  10.6 0.0 all-gather.7.cloned.1.call-update
  10.6 0.0 all-gather.9.cloned.1.call-start
  10.7 12.0 %all_gather.20 = bf16[256,512]{1,0:T(8,128)(2,1)} all-gather(bf16[256,128]{1,0:T(8,128)(2,1)} %param.20), channel_id=1, replica_groups=mesh['sp_0'=8,'sp_1'=4,'tp'=8] {'sp_1'}, dimensions={1}, use_global_device_ids=true | all-gather | bytes 327680 | tf_op jit(solution)/shard_map/all_gather | solution.py:43
  22.7 0.0 all-gather.9.cloned.1.call-update
  22.7 0.0 all-gather.11.cloned.1.call-start
  22.7 11.1 %all_gather.22 = bf16[256,512]{1,0:T(8,128)(2,1)} all-gather(bf16[256,128]{1,0:T(8,128)(2,1)} %param.21), channel_id=1, replica_groups=mesh['sp_0'=8,'sp_1'=4,'tp'=8] {'sp_1'}, dimensions={1}, use_global_device_ids=true | all-gather | bytes 327680 | tf_op jit(solution)/shard_map/all_gather | solution.py:43
  33.8 0.0 all-gather.11.cloned.1.call-update
  33.8 0.0 copy-start.13
  33.8 0.0 reduce-scatter.2.cloned.1.call-start
  34.0 0.6 broadcast_compare_fusion
  34.6 0.6 broadcast_compare_fusion.2
  35.2 0.1 broadcast_multiply_fusion.1
  35.3 0.5 fusion.76
  35.7 3.1 fusion.7
  38.8 26.8 %all-gather.5.cloned.1.call-done = bf16[1024,4096]{1,0:T(8,128)(2,1)} async-done(((bf16[1024,512]{1,0:T(8,128)(2,1)}), bf16[1024,4096]{1,0:T(8,128)(2,1)}) %all-gather.5.cloned.1.call-update) | async-done | bytes 8388624 | tf_op jit(solution)/shard_map/all_gather | solution.py:86
  65.6 5.1 %fusion.1 = f32[1024]{0:T(1024)S(1)} fusion(bf16[1024,4096]{1,0:T(8,128)(2,1)} %all-gather.5.cloned.1.call-done), kind=kLoop, calls=%fused_computation.6 | loop fusion | flops 12581888 | bytes 8392704 | tf_op jit(solution)/shard_map/reduce_sum | solution.py:49
  70.7 10.3 %fusion.3 = bf16[1024,4096]{1,0:T(8,128)(2,1)} fusion(bf16[1024,4096]{1,0:T(8,128)(2,1)} %all-gather.5.cloned.1.call-done, f32[4096]{0:T(1024)S(1)} %copy-done.13, f32[1024]{0:T(1024)S(1)} %add_rsqrt_fusion), kind=kLoop, calls=%fused_computation.8 | loop fusion | flops 16777216 | bytes 16797696 | tf_op jit(solution)/shard_map/convert_element_type | solution.py:50
  81.0 68.8 %all-gather.7.cloned.1.call-done = bf16[4096,640]{1,0:T(8,128)(2,1)} async-done(((bf16[128,640]{1,0:T(8,128)(2,1)}), bf16[4096,640]{1,0:T(8,128)(2,1)}) %all-gather.7.cloned.1.call-update) | async-done | bytes 5242896 | tf_op jit(solution)/shard_map/all_gather | solution.py:23
  149.9 6.4 %fusion.33 = f32[1024,64]{0,1:T(8,128)S(1)} fusion(bf16[1024,4096]{1,0:T(8,128)(2,1)} %fusion.3, bf16[4096,640]{1,0:T(8,128)(2,1)} %all-gather.7.cloned.1.call-done), kind=kOutput, calls=%fused_computation.42 | convolution fusion | flops 536870912 | bytes 9699328 | tf_op jit(solution)/shard_map/dot_general | solution.py:91
  156.3 0.5 subtract_convert_fusion.1
  156.8 0.6 copy-done.8
  157.4 2.4 fusion.14
  159.8 0.0 copy-start.4
  159.8 2.7 convolution_convert_fusion
  162.6 1.9 collective-permute-start
  164.5 1.5 collective-permute-start.1
  166.0 2.4 fusion.8
  168.4 0.2 subtract_convert_fusion
  168.5 0.8 pad_maximum_fusion.1
  169.4 0.0 collective-permute-done
  169.4 0.9 collective-permute-done.1
  170.3 0.1 pad_maximum_fusion
  170.4 0.5 copy-done.11
  170.9 0.2 slice_bitcast_fusion
  171.2 0.1 pad_convert_fusion
  171.2 0.4 copy.19
  171.6 1.3 fusion.12
  172.9 0.2 broadcast_add_fusion
  173.2 0.0 copy-start.14
  173.2 5.2 %fusion.96 = (f32[4,1024]{1,0:T(4,128)S(1)}, f32[1,4,1024,1280]{2,3,1,0:T(8,128)S(1)}) fusion(bf16[1024,4,64]{0,2,1:T(8,128)(2,1)} %bitcast.62, bf16[128,384]{0,1:T(8,128)(2,1)} %copy-done.11, bf16[128,384]{0,1:T(8,128)(2,1)} %copy-done.9, bf16[1024,64]{0,1:T(8,128)(2,1)S(1)} %convolution_convert_fusion, bf16[1024,64]{0,1:T(8,128)(2,1)} %bitcast.59, ...), kind=kOutput, calls=%fused_computation.140 | convolution fusion | flops 687632384 | bytes 23805952 | tf_op jit(solution)/shard_map/qkgd,skd->kgqs/dot_general | solution.py:144
  178.4 0.0 copy-start.3
  178.4 0.0 copy-done.14
  178.4 0.1 broadcast_maximum_fusion
  178.5 3.0 fusion
  181.5 4.0 %copy-done.3 = f32[1,4,1024,1280]{2,3,1,0:T(8,128)} copy-done((f32[1,4,1024,1280]{2,3,1,0:T(8,128)}, f32[1,4,1024,1280]{2,3,1,0:T(8,128)S(1)}, u32[]{:S(2)}) %copy-start.3) | copy-done | bytes 20971544
  185.5 0.1 exponential_add_fusion
  185.6 0.7 copy.21
  186.3 0.4 copy.22
  186.7 3.0 all-gather.9.cloned.1.call-done
  189.7 0.0 copy-done.5
  189.7 0.0 copy-done.16
  189.8 10.7 %fusion.21 = f32[1024,4096]{1,0:T(8,128)} fusion(bf16[256,4096]{1,0:T(8,128)(2,1)} %all-gather.9.cloned.1.call-done, bf16[1024,256]{0,1:T(8,128)(2,1)S(1)} %copy-done.5, f32[1152,256]{0,1:T(8,128)S(1)} %bitcast.55, f32[1040,256]{0,1:T(8,128)S(1)} %bitcast.56, f32[256]{0:T(256)S(1)} %copy-done.15, f32[1024]{0:T(1024)S(1)} %get-tuple-element.23, ...), kind=kOutput, calls=%fused_computation.25 | convolution fusion | flops 2286157824 | bytes 28068864 | tf_op jit(solution)/shard_map/dot_general | solution.py:167
  200.5 9.3 %fusion.18 = bf16[64,4,1024]{2,0,1:T(8,128)(2,1)S(1)} fusion(f32[4,1024]{1,0:T(4,128)S(1)} %exponential_add_fusion, f32[1,4,1024,1280]{2,3,1,0:T(8,128)} %copy-done.3, f32[4,1024]{1,0:T(4,128)S(1)} %broadcast_maximum_fusion, bf16[128,384]{0,1:T(8,128)(2,1)S(1)} %copy-done.12, bf16[128,384]{0,1:T(8,128)(2,1)S(1)} %copy-done.10, ...), kind=kOutput, calls=%fused_computation.24 | convolution fusion | flops 687898624 | bytes 22511616 | tf_op jit(solution)/shard_map/kgqs,skd->qkgd/dot_general | solution.py:159
  209.8 20.3 %all-gather.11.cloned.1.call-done = bf16[256,4096]{1,0:T(8,128)(2,1)} async-done(((bf16[256,512]{1,0:T(8,128)(2,1)}), bf16[256,4096]{1,0:T(8,128)(2,1)}) %all-gather.11.cloned.1.call-update) | async-done | bytes 2097168 | tf_op jit(solution)/shard_map/all_gather | solution.py:43
  230.1 12.1 %add_convert_fusion = bf16[1024,4096]{1,0:T(8,128)(2,1)} fusion(f32[1024,4096]{1,0:T(8,128)} %fusion.21, bf16[1024,256]{0,1:T(8,128)(2,1)S(1)} %bitcast.54, bf16[256,4096]{1,0:T(8,128)(2,1)} %all-gather.11.cloned.1.call-done), kind=kOutput, calls=%fused_computation.9 | convolution fusion | flops 2155872256 | bytes 27787264 | tf_op jit(solution)/shard_map/dot_general | solution.py:168
  242.2 0.0 reduce-scatter.2.cloned.1.call-update
  242.2 57.4 %reduce-scatter.2.cloned.1.call-done = bf16[128,4096]{1,0:T(8,128)(2,1)} async-done(((bf16[1024,4096]{1,0:T(8,128)(2,1)}), bf16[128,4096]{1,0:T(8,128)(2,1)}) %reduce-scatter.2.cloned.1.call-update) | async-done | bytes 1048592 | tf_op jit(solution)/shard_map/reduce_scatter | solution.py:165
  (41 shorter events, 0.2 us)
Async XLA Ops:
  6.5 183.2 %copy-start = (bf16[1,256,256]{2,1,0:T(8,128)(2,1)S(1)}, bf16[1,256,256]{2,1,0:T(8,128)(2,1)}, u32[]{:S(2)}) copy-start(bf16[1,256,256]{2,1,0:T(8,128)(2,1)} %param.17) | copy-start | bytes 393220
  6.5 59.1 %all-gather.5.cloned.1.call-start = ((), (), s32[]{:S(2)}) async-start(), calls=%async_computation.1 | async-start | bytes 9437184 | tf_op jit(solution)/shard_map/all_gather | solution.py:86
  7.3 142.6 %all-gather.7.cloned.1.call-start = ((), (), s32[]{:S(2)}) async-start(), calls=%async_computation.2 | async-start | bytes 5406720 | tf_op jit(solution)/shard_map/all_gather | solution.py:23
  10.6 179.1 %all-gather.9.cloned.1.call-start = ((), (), s32[]{:S(2)}) async-start(), calls=%async_computation.3 | async-start | bytes 2359296 | tf_op jit(solution)/shard_map/all_gather | solution.py:43
  22.7 207.4 %all-gather.11.cloned.1.call-start = ((), (), s32[]{:S(2)}) async-start(), calls=%async_computation.4 | async-start | bytes 2359296 | tf_op jit(solution)/shard_map/all_gather | solution.py:43
  33.8 36.9 %copy-start.13 = (f32[4096]{0:T(1024)S(1)}, f32[4096]{0:T(1024)}, u32[]{:S(2)}) copy-start(f32[4096]{0:T(1024)} %param.12) | copy-start | bytes 49156
  33.8 265.8 %reduce-scatter.2.cloned.1.call-start = ((), (), s32[]{:S(2)}) async-start(), calls=%async_computation.5 | async-start | bytes 9437184 | tf_op jit(solution)/shard_map/reduce_scatter | solution.py:165
  149.8 6.9 %copy-start.2 = (bf16[1024,4096]{1,0:T(8,128)(2,1)S(1)}, bf16[1024,4096]{1,0:T(8,128)(2,1)}, u32[]{:S(2)}) copy-start(bf16[1024,4096]{1,0:T(8,128)(2,1)} %fusion.3) | copy-start | bytes 25165828
  149.9 7.6 %copy-start.8 = (bf16[4096,640]{1,0:T(8,128)(2,1)S(1)}, bf16[4096,640]{1,0:T(8,128)(2,1)}, u32[]{:S(2)}) copy-start(bf16[4096,640]{1,0:T(8,128)(2,1)} %all-gather.7.cloned.1.call-done) | copy-start | bytes 15728644
  157.4 12.8 %copy-start.6 = (bf16[1024,1,2,2,16]{0,4,3,2,1:T(8,128)(2,1)}, bf16[1024,1,2,2,16]{0,4,3,2,1:T(8,128)(2,1)S(1)}, u32[]{:S(2)}) copy-start(bf16[1024,1,2,2,16]{0,4,3,2,1:T(8,128)(2,1)S(1)} %pad_maximum_fusion.4) | copy-start | bytes 393220
  159.8 10.4 %copy-start.4 = (bf16[1024,256]{0,1:T(8,128)(2,1)}, bf16[1024,256]{0,1:T(8,128)(2,1)S(1)}, u32[]{:S(2)}) copy-start(bf16[1024,256]{0,1:T(8,128)(2,1)S(1)} %fusion.14) | copy-start | bytes 1572868
  162.6 6.8 %collective-permute-start = (bf16[128,384]{0,1:T(8,128)(2,1)S(1)}, bf16[128,384]{0,1:T(8,128)(2,1)S(1)}, u32[]{:S(2)}, u32[]{:S(2)}) collective-permute-start(bf16[128,384]{0,1:T(8,128)(2,1)S(1)} %get-tuple-element.7), channel_id=1, source_target_pairs={{0,8},{8,16},{16,24},{24,32},{32,40},{40,48},{48,56},{56,64},{64,7... | collective-permute-start | bytes 294920 | tf_op jit(solution)/shard_map/ppermute | solution.py:32
  164.5 5.8 %collective-permute-start.1 = (bf16[128,384]{0,1:T(8,128)(2,1)S(1)}, bf16[128,384]{0,1:T(8,128)(2,1)S(1)}, u32[]{:S(2)}, u32[]{:S(2)}) collective-permute-start(bf16[128,384]{0,1:T(8,128)(2,1)S(1)} %get-tuple-element.8), channel_id=1, source_target_pairs={{8,0},{16,8},{24,16},{32,24},{40,32},{48,40},{56,48},{64,56},{72,6... | collective-permute-start | bytes 294920 | tf_op jit(solution)/shard_map/ppermute | solution.py:35
  169.4 1.0 copy-start.9
  170.3 0.6 copy-start.11
  173.2 5.2 %copy-start.14 = (f32[4]{0:T(128)S(1)}, f32[4]{0:T(128)}, u32[]{:S(2)}) copy-start(f32[4]{0:T(128)} %param.19) | copy-start | bytes 52
  178.4 7.1 %copy-start.3 = (f32[1,4,1024,1280]{2,3,1,0:T(8,128)}, f32[1,4,1024,1280]{2,3,1,0:T(8,128)S(1)}, u32[]{:S(2)}) copy-start(f32[1,4,1024,1280]{2,3,1,0:T(8,128)S(1)} %get-tuple-element.20) | copy-start | bytes 62914564
  185.5 4.2 %copy-start.5 = (bf16[1024,256]{0,1:T(8,128)(2,1)S(1)}, bf16[1024,256]{0,1:T(8,128)(2,1)}, u32[]{:S(2)}) copy-start(bf16[1024,256]{0,1:T(8,128)(2,1)} %copy-done.4) | copy-start | bytes 1572868
  185.5 4.2 %copy-start.15 = (f32[256]{0:T(256)S(1)}, f32[256]{0:T(256)}, u32[]{:S(2)}) copy-start(f32[256]{0:T(256)} %param.18) | copy-start | bytes 3076
  185.5 4.2 %copy-start.16 = (pred[256]{0:T(512)(128)(4,1)S(1)}, pred[256]{0:T(512)(128)(4,1)}, u32[]{:S(2)}) copy-start(pred[256]{0:T(512)(128)(4,1)} %get-tuple-element.27) | copy-start | bytes 772
  185.5 4.2 %copy-start.17 = (pred[256]{0:T(512)(128)(4,1)S(1)}, pred[256]{0:T(512)(128)(4,1)}, u32[]{:S(2)}) copy-start(pred[256]{0:T(512)(128)(4,1)} %get-tuple-element.28) | copy-start | bytes 772
  185.6 4.2 %copy-start.18 = (pred[256]{0:T(512)(128)(4,1)S(1)}, pred[256]{0:T(512)(128)(4,1)}, u32[]{:S(2)}) copy-start(pred[256]{0:T(512)(128)(4,1)} %get-tuple-element.29) | copy-start | bytes 772
  185.6 4.2 %copy-start.19 = (pred[256]{0:T(512)(128)(4,1)S(1)}, pred[256]{0:T(512)(128)(4,1)}, u32[]{:S(2)}) copy-start(pred[256]{0:T(512)(128)(4,1)} %get-tuple-element.30) | copy-start | bytes 772
  189.8 10.7 %copy-start.7 = (bf16[1024,1,2,2,16]{0,4,3,2,1:T(8,128)(2,1)S(1)}, bf16[1024,1,2,2,16]{0,4,3,2,1:T(8,128)(2,1)}, u32[]{:S(2)}) copy-start(bf16[1024,1,2,2,16]{0,4,3,2,1:T(8,128)(2,1)} %copy-done.6) | copy-start | bytes 393220
  189.8 10.7 %copy-start.10 = (bf16[128,384]{0,1:T(8,128)(2,1)S(1)}, bf16[128,384]{0,1:T(8,128)(2,1)}, u32[]{:S(2)}) copy-start(bf16[128,384]{0,1:T(8,128)(2,1)} %copy-done.9) | copy-start | bytes 294916
  189.8 10.7 %copy-start.12 = (bf16[128,384]{0,1:T(8,128)(2,1)S(1)}, bf16[128,384]{0,1:T(8,128)(2,1)}, u32[]{:S(2)}) copy-start(bf16[128,384]{0,1:T(8,128)(2,1)} %copy-done.11) | copy-start | bytes 294916
  230.1 69.5 %copy-start.1 = (bf16[1,256,256]{2,1,0:T(8,128)(2,1)S(1)}, bf16[1,256,256]{2,1,0:T(8,128)(2,1)}, u32[]{:S(2)}) copy-start(bf16[1,256,256]{2,1,0:T(8,128)(2,1)} %param.17) | copy-start | bytes 393220
Sparse Core Ops, SparseCore 0:
  9.2 56.4 all-gather.4
  68.2 81.6 all-gather.6
  151.6 38.0 all-gather.8
  191.4 38.6 all-gather.10
  242.3 57.2 reduce-scatter.1
where the time goes:
time: 307 us; the launch traced here: 306 us
  waiting for transfers between devices  178 us (58%)
  matrix products  51.3 us (17%)
  other arithmetic  28.3 us (9%)
  blocking collectives  23 us (7%)
  between operations  13.5 us (4%)
  local copies, waits for them, and re-layouts  8.52 us (3%)
  starting transfers between devices  3.52 us (1%)
    all_gather x1, waiting for transfers between devices, sent_together(): result = lax.all_gather(both, axis, axis=dim, tiled=True)  68.8 us
    reduce_scatter x1, waiting for transfers between devices, shards(): lax.psum_scatter((jnp.dot(pool_out, out_pool_full, preferred_element_type...  57.4 us
    all_gather x1, waiting for transfers between devices, shards(): whole_rows = lax.all_gather(tokens, 'tp', axis=1, tiled=True)  26.8 us
    all_gather x2, waiting for transfers between devices, gather_axes(): nearer = lax.all_gather(array, axes[-1], axis=dim, tiled=True)  23.3 us
    all_gather x2, blocking collectives, gather_axes(): nearer = lax.all_gather(array, axes[-1], axis=dim, tiled=True)  23 us
    dot_general x4, matrix products, project(): return jnp.dot(normed, piece, preferred_element_type=jnp.float32)  13.9 us
    dot_general x1, matrix products, shards(): jnp.dot(attn_out, out_attn_full, preferred_element_type=jnp.float32)  12.1 us
    dot_general x1, matrix products, shards(): jnp.dot(pool_out, out_pool_full, preferred_element_type=jnp.float32)  10.7 us
  transfers between devices with their start and end apart: 7, of which 6 were waited for; matrix products, arithmetic and copies ran while one was open for 23% of the time, Pallas kernels for 0%

commit v1 on v0

--- a/solution.py
+++ b/solution.py
@@ -83,7 +83,11 @@
     out_pool_weight,
     out_attn_weight,
 ):
-    whole_rows = lax.all_gather(tokens, "tp", axis=1, tiled=True)
+    count_2 = lax.axis_size("tp")
+    repeats = [count_2 if d == 1 else 1 for d in range(tokens.ndim)]
+    whole_rows = lax.all_to_all(
+        jnp.tile(tokens, repeats), "tp", split_axis=1, concat_axis=1, tiled=True
+    )
     normed = rms_normed(whole_rows, norm_gain)
     tok_rows = normed.shape[0]
 

time: 307 us -> 286 us (0.932)
  waiting for transfers between devices: 178 us -> 128 us
  local copies, waits for them, and re-layouts: 8.52 us -> 31.4 us
  starting transfers between devices: 3.52 us -> 11.3 us
    all_gather x1, waiting for transfers between devices: 68.8 us -> 0.01 us  [sent_together(): result = lax.all_gather(both, axis, axis=dim, tiled=True)]
    all_to_all x0 -> x1, waiting for transfers between devices: none -> 67.3 us  [shards(): lax.all_to_all(jnp.tile(tokens, repeats), 'tp', split_axis=1, concat_axis...]
    all_gather x1 -> x0, waiting for transfers between devices: 26.8 us -> none  [shards(): whole_rows = lax.all_gather(tokens, 'tp', axis=1, tiled=True)]
    all_gather x2, waiting for transfers between devices: 23.3 us -> 0.04 us  [gather_axes(): nearer = lax.all_gather(array, axes[-1], axis=dim, tiled=True)]
    all_to_all x0 -> x1, local copies, waits for them, and re-layouts: none -> 11.6 us  [shards(): lax.all_to_all(jnp.tile(tokens, repeats), 'tp', split_axis=1, concat_axis...]
    all_to_all x0 -> x1, starting transfers between devices: none -> 8.17 us  [shards(): lax.all_to_all(jnp.tile(tokens, repeats), 'tp', split_axis=1, concat_axis...]
    dot_general x0 -> x4, local copies, waits for them, and re-layouts: none -> 6.36 us  [project(): return jnp.dot(normed, piece, preferred_element_type=jnp.float32)]
    another operation x5 -> x6, local copies, waits for them, and re-layouts: 1.67 us -> 6.86 us  [the longest x1 5.19 us: shards(): jnp.tile(tokens, repeats)]
  transfers between devices with their start and end apart: 7 -> 7, of which waited for: 6 -> 3; matrix products, arithmetic and copies ran while one was open for 23% -> 32% of each run, Pallas kernels for 0% -> 0%
where the time goes in v1:
time: 286 us; the launch traced here: 285 us
  waiting for transfers between devices  128 us (45%)
  matrix products  52.6 us (18%)
  local copies, waits for them, and re-layouts  31.4 us (11%)
  other arithmetic  26.9 us (9%)
  blocking collectives  21.2 us (7%)
  between operations  13.7 us (5%)
  starting transfers between devices  11.3 us (4%)
    all_to_all x1, waiting for transfers between devices, shards(): lax.all_to_all(jnp.tile(tokens, repeats), 'tp', split_axis=1, concat_axis...  67.3 us
    reduce_scatter x1, waiting for transfers between devices, shards(): lax.psum_scatter((jnp.dot(pool_out, out_pool_full, preferred_element_type...  59.2 us
    all_gather x2, blocking collectives, gather_axes(): nearer = lax.all_gather(array, axes[-1], axis=dim, tiled=True)  21.2 us
    dot_general x4, matrix products, project(): return jnp.dot(normed, piece, preferred_element_type=jnp.float32)  15.5 us
    dot_general x1, matrix products, shards(): jnp.dot(attn_out, out_attn_full, preferred_element_type=jnp.float32)  12.1 us
    all_to_all x1, local copies, waits for them, and re-layouts, shards(): lax.all_to_all(jnp.tile(tokens, repeats), 'tp', split_axis=1, concat_axis...  11.6 us
    dot_general x1, matrix products, shards(): jnp.dot(pool_out, out_pool_full, preferred_element_type=jnp.float32)  10.7 us
    dot_general x1, matrix products, shards(): jnp.einsum('kgqs,skd->qkgd', weights, value_pad, preferred_element_type=j...  9.21 us
  transfers between devices with their start and end apart: 7, of which 3 were waited for; matrix products, arithmetic and copies ran while one was open for 32% of the time, Pallas kernels for 0%

profile of v1, /device:TPU:1, one launch (start us, length us, event | category | flops | bytes accessed | tf_op | source)
XLA Modules:
  0.0 284.7 jit_solution(9733461760105701471)
XLA Ops:
  6.5 0.9 copy.38
  7.4 0.8 copy.39
  8.2 1.6 pad_maximum_fusion.2
  9.9 0.0 all-gather.4.cloned.1.call-update
  9.9 5.2 %tile.2 = bf16[1024,8,512]{2,0,1:T(8,128)(2,1)} broadcast(bf16[1024,512]{1,0:T(8,128)(2,1)} %param.11), dimensions={0,2} | broadcast | bytes 9437184 | tf_op jit(solution)/shard_map/tile | solution.py:89
  15.1 8.2 %all-to-all-start = ((bf16[1024,8,512]{2,0,1:T(8,128)(2,1)}), bf16[1024,8,512]{2,0,1:T(8,128)(2,1)}, u32[]{:S(2)}, u32[]{:S(2)}) async-start(bf16[1024,8,512]{2,0,1:T(8,128)(2,1)} %tile.2), calls=%async_computation | async-start | bytes 16777216 | tf_op jit(solution)/shard_map/all_to_all | solution.py:88
  23.3 10.3 %all_gather.16 = bf16[256,512]{1,0:T(8,128)(2,1)} all-gather(bf16[256,128]{1,0:T(8,128)(2,1)S(1)} %copy-done.12), channel_id=1, replica_groups=mesh['sp_0'=8,'sp_1'=4,'tp'=8] {'sp_1'}, dimensions={1}, use_global_device_ids=true | all-gather | bytes 327680 | tf_op jit(solution)/shard_map/all_gather | solution.py:43
  33.6 0.0 all-gather.6.cloned.1.call-update
  33.6 0.0 all-gather.8.cloned.1.call-start
  33.7 10.9 %all_gather.18 = bf16[256,512]{1,0:T(8,128)(2,1)} all-gather(bf16[256,128]{1,0:T(8,128)(2,1)S(1)} %copy-done.13), channel_id=1, replica_groups=mesh['sp_0'=8,'sp_1'=4,'tp'=8] {'sp_1'}, dimensions={1}, use_global_device_ids=true | all-gather | bytes 327680 | tf_op jit(solution)/shard_map/all_gather | solution.py:43
  44.6 0.0 all-gather.8.cloned.1.call-update
  44.6 0.0 reduce-scatter.2.cloned.1.call-start
  44.7 0.6 broadcast_compare_fusion
  45.3 0.6 broadcast_compare_fusion.2
  46.0 0.1 broadcast_multiply_fusion.1
  46.1 0.5 fusion.71
  46.5 3.1 %fusion.6 = pred[1024,1280]{0,1:T(8,128)(4,1)} fusion(s32[1024]{0:T(1024)S(1)} %iota_add_fusion.1, s32[1280]{0:T(1024)S(1)} %iota_add_fusion, pred[1280]{0:T(1024)(128)(4,1)S(1)} %get-tuple-element.31, pred[1280]{0:T(1024)(128)(4,1)S(1)} %get-tuple-element.32), kind=kLoop, calls=%fused_computation.14 | loop fusion | flops 6553600 | bytes 1322496 | tf_op jit(solution)/shard_map/and | solution.py:153
  49.7 67.3 %all-to-all-done = bf16[1024,8,512]{2,0,1:T(8,128)(2,1)} async-done(((bf16[1024,8,512]{2,0,1:T(8,128)(2,1)}), bf16[1024,8,512]{2,0,1:T(8,128)(2,1)}, u32[]{:S(2)}, u32[]{:S(2)}) %all-to-all-start) | async-done | bytes 8388640 | tf_op jit(solution)/shard_map/all_to_all | solution.py:88
  117.0 11.6 %copy.37 = bf16[1024,8,512]{0,2,1:T(8,128)(2,1)} copy(bf16[1024,8,512]{2,0,1:T(8,128)(2,1)} %all-to-all-done) | data formatting | bytes 16777216 | tf_op jit(solution)/shard_map/all_to_all | solution.py:88
  128.6 5.3 %multiply_reduce_fusion = f32[1024]{0:T(1024)S(1)} fusion(bf16[1024,8,512]{0,2,1:T(8,128)(2,1)} %copy.37), kind=kLoop, calls=%fused_computation.9 | loop fusion | flops 12581888 | bytes 8392704 | tf_op jit(solution)/shard_map/reduce_sum | solution.py:49
  133.9 0.6 copy-done.1
  134.4 4.4 %fusion.2 = bf16[1024,4096]{0,1:T(8,128)(2,1)} fusion(bf16[1024,8,512]{0,2,1:T(8,128)(2,1)S(1)} %copy-done.1, f32[4096]{0:T(1024)S(1)} %copy-done.14, f32[1024]{0:T(1024)S(1)} %add_rsqrt_fusion), kind=kLoop, calls=%fused_computation.6 | loop fusion | flops 16777216 | bytes 16797696 | tf_op jit(solution)/shard_map/convert_element_type | solution.py:50
  138.8 4.3 %multiply_convert_fusion = bf16[1024,8,512]{0,2,1:T(8,128)(2,1)} fusion(bf16[1024,8,512]{0,2,1:T(8,128)(2,1)S(1)} %copy-done.1, f32[8,512]{1,0:T(8,128)S(1)} %mul.187, f32[1024]{0:T(1024)S(1)} %add_rsqrt_fusion), kind=kLoop, calls=%fused_computation.8 | loop fusion | flops 16777216 | bytes 16797696 | tf_op jit(solution)/shard_map/convert_element_type | solution.py:50
  143.1 1.7 slice_bitcast_fusion
  144.8 3.0 %copy.46 = bf16[256,4096]{1,0:T(8,128)(2,1)} copy(bf16[256,4096]{0,1:T(8,128)(2,1)S(1)} %slice_bitcast_fusion) | data formatting | bytes 4194304 | tf_op jit(solution)/shard_map/dot_general | solution.py:95
  147.9 1.3 slice_bitcast_fusion.1
  149.2 0.0 slice-start.4
  149.2 0.3 copy.40
  149.5 0.0 slice-start.5
  149.5 5.2 %convolution_bitcast_fusion = f32[1024,1,2,2,16]{0,4,3,2,1:T(8,128)S(1)} fusion(bf16[1024,4096,1,1]{0,1,3,2:T(8,128)(2,1)} %bitcast.70, bf16[2,2,16,4096]{3,2,1,0:T(8,128)(2,1)S(1)} %bitcast.88), kind=kOutput, calls=%fused_computation.26 | convolution fusion | flops 536870912 | bytes 9175040 | tf_op jit(solution)/shard_map/dot_general | solution.py:95
  154.7 0.5 subtract_convert_fusion.1
  155.2 0.0 slice-start.3
  155.2 0.0 slice-start.1
  155.3 6.1 %fusion.11 = bf16[1024,256]{0,1:T(8,128)(2,1)S(1)} fusion(bf16[1024,4096]{0,1:T(8,128)(2,1)} %fusion.2, bf16[4096,640]{1,0:T(8,128)(2,1)S(1)} %bitcast.80), kind=kOutput, calls=%fused_computation.21 | convolution fusion | flops 2147745792 | bytes 11010048 | tf_op jit(solution)/shard_map/dot_general | solution.py:95
  161.4 0.0 copy-start.4
  161.4 2.0 convolution_convert_fusion
  163.4 1.6 collective-permute-start
  165.0 1.5 collective-permute-start.1
  166.5 2.3 fusion.92
  168.8 0.1 subtract_convert_fusion
  169.0 0.8 pad_maximum_fusion.1
  169.8 0.9 collective-permute-done.1
  170.8 0.1 pad_maximum_fusion
  170.8 0.2 slice_bitcast_fusion.2
  171.1 0.3 copy-done.10
  171.4 0.1 pad_convert_fusion
  171.5 0.4 copy.42
  171.8 1.3 fusion.9
  173.2 0.2 broadcast_add_fusion
  173.4 0.0 copy-start.15
  173.4 5.1 %fusion.91 = (f32[4,1024]{1,0:T(4,128)S(1)}, f32[1,4,1024,1280]{2,3,1,0:T(8,128)S(1)}) fusion(bf16[1024,4,64]{0,2,1:T(8,128)(2,1)} %bitcast.89, bf16[128,384]{0,1:T(8,128)(2,1)} %copy-done.10, bf16[128,384]{0,1:T(8,128)(2,1)} %copy-done.8, bf16[1024,64]{0,1:T(8,128)(2,1)} %copy-done.6, bf16[1024,64]{0,1:T(8,128)(2,1)S(1)} %bitcast.86, ...), kind=kOutput, calls=%fused_computation.139 | convolution fusion | flops 687632384 | bytes 23805952 | tf_op jit(solution)/shard_map/qkgd,skd->kgqs/dot_general | solution.py:148
  178.6 0.1 broadcast_maximum_fusion
  178.7 3.0 %fusion = f32[4,1024]{1,0:T(4,128)S(1)} fusion(f32[1,4,1024,1280]{2,3,1,0:T(8,128)S(1)} %get-tuple-element.20, f32[4,1024]{1,0:T(4,128)S(1)} %broadcast_maximum_fusion), kind=kLoop, calls=%fused_computation.3 | loop fusion | flops 10481664 | bytes 21004288 | tf_op jit(solution)/shard_map/reduce_sum | solution.py:161
  181.7 3.9 %copy-done.2 = f32[1,4,1024,1280]{2,3,1,0:T(8,128)} copy-done((f32[1,4,1024,1280]{2,3,1,0:T(8,128)}, f32[1,4,1024,1280]{2,3,1,0:T(8,128)S(1)}, u32[]{:S(2)}) %copy-start.2) | copy-done | bytes 20971544
  185.6 0.1 exponential_add_fusion
  185.7 0.7 copy.44
  186.4 0.4 copy.45
  186.8 0.0 all-gather.6.cloned.1.call-done
  186.9 10.7 %fusion.18 = f32[1024,4096]{1,0:T(8,128)} fusion(bf16[256,4096]{1,0:T(8,128)(2,1)} %all-gather.6.cloned.1.call-done, bf16[1024,256]{0,1:T(8,128)(2,1)S(1)} %copy-done.5, f32[1152,256]{0,1:T(8,128)S(1)} %bitcast.82, f32[1040,256]{0,1:T(8,128)S(1)} %bitcast.83, f32[256]{0:T(256)S(1)} %copy-done.16, f32[1024]{0:T(1024)S(1)} %get-tuple-element.23, ...), kind=kOutput, calls=%fused_computation.24 | convolution fusion | flops 2286157824 | bytes 28068864 | tf_op jit(solution)/shard_map/dot_general | solution.py:171
  197.6 9.2 %fusion.15 = bf16[64,4,1024]{2,0,1:T(8,128)(2,1)S(1)} fusion(f32[4,1024]{1,0:T(4,128)S(1)} %exponential_add_fusion, f32[1,4,1024,1280]{2,3,1,0:T(8,128)} %copy-done.2, f32[4,1024]{1,0:T(4,128)S(1)} %broadcast_maximum_fusion, bf16[128,384]{0,1:T(8,128)(2,1)S(1)} %copy-done.11, bf16[128,384]{0,1:T(8,128)(2,1)S(1)} %copy-done.9, ...), kind=kOutput, calls=%fused_computation.23 | convolution fusion | flops 687898624 | bytes 22511616 | tf_op jit(solution)/shard_map/kgqs,skd->qkgd/dot_general | solution.py:163
  206.8 0.0 all-gather.8.cloned.1.call-done
  206.9 12.1 %add_convert_fusion = bf16[1024,4096]{1,0:T(8,128)(2,1)} fusion(f32[1024,4096]{1,0:T(8,128)} %fusion.18, bf16[1024,256]{0,1:T(8,128)(2,1)S(1)} %bitcast.81, bf16[256,4096]{1,0:T(8,128)(2,1)} %all-gather.8.cloned.1.call-done), kind=kOutput, calls=%fused_computation.7 | convolution fusion | flops 2155872256 | bytes 27787264 | tf_op jit(solution)/shard_map/dot_general | solution.py:172
  219.0 0.0 reduce-scatter.2.cloned.1.call-update
  219.0 59.2 %reduce-scatter.2.cloned.1.call-done = bf16[128,4096]{1,0:T(8,128)(2,1)} async-done(((bf16[1024,4096]{1,0:T(8,128)(2,1)}), bf16[128,4096]{1,0:T(8,128)(2,1)}) %reduce-scatter.2.cloned.1.call-update) | async-done | bytes 1048592 | tf_op jit(solution)/shard_map/reduce_scatter | solution.py:169
  (65 shorter events, 0.2 us)
Async XLA Ops:
  6.5 180.3 %copy-start = (bf16[1,256,256]{2,1,0:T(8,128)(2,1)S(1)}, bf16[1,256,256]{2,1,0:T(8,128)(2,1)}, u32[]{:S(2)}) copy-start(bf16[1,256,256]{2,1,0:T(8,128)(2,1)} %param.17) | copy-start | bytes 393220
  6.5 136.6 %all-gather.4.cloned.1.call-start = ((), (), s32[]{:S(2)}) async-start(), calls=%async_computation.2 | async-start | bytes 5406720 | tf_op jit(solution)/shard_map/all_gather | solution.py:23
  15.1 8.2 %copy-start.12 = (bf16[256,128]{1,0:T(8,128)(2,1)S(1)}, bf16[256,128]{1,0:T(8,128)(2,1)}, u32[]{:S(2)}) copy-start(bf16[256,128]{1,0:T(8,128)(2,1)} %param.20) | copy-start | bytes 196612
  15.1 18.6 %copy-start.13 = (bf16[256,128]{1,0:T(8,128)(2,1)S(1)}, bf16[256,128]{1,0:T(8,128)(2,1)}, u32[]{:S(2)}) copy-start(bf16[256,128]{1,0:T(8,128)(2,1)} %param.21) | copy-start | bytes 196612
  15.1 29.6 %copy-start.14 = (f32[4096]{0:T(1024)S(1)}, f32[4096]{0:T(1024)}, u32[]{:S(2)}) copy-start(f32[4096]{0:T(1024)} %param.12) | copy-start | bytes 49156
  15.1 101.9 %all-to-all-start = ((bf16[1024,8,512]{2,0,1:T(8,128)(2,1)}), bf16[1024,8,512]{2,0,1:T(8,128)(2,1)}, u32[]{:S(2)}, u32[]{:S(2)}) async-start(bf16[1024,8,512]{2,0,1:T(8,128)(2,1)} %tile.2), calls=%async_computation | async-start | bytes 16777216 | tf_op jit(solution)/shard_map/all_to_all | solution.py:88
  23.3 163.5 %all-gather.6.cloned.1.call-start = ((), (), s32[]{:S(2)}) async-start(), calls=%async_computation.3 | async-start | bytes 2359296 | tf_op jit(solution)/shard_map/all_gather | solution.py:43
  33.6 173.2 %all-gather.8.cloned.1.call-start = ((), (), s32[]{:S(2)}) async-start(), calls=%async_computation.4 | async-start | bytes 2359296 | tf_op jit(solution)/shard_map/all_gather | solution.py:43
  44.6 233.6 %reduce-scatter.2.cloned.1.call-start = ((), (), s32[]{:S(2)}) async-start(), calls=%async_computation.5 | async-start | bytes 9437184 | tf_op jit(solution)/shard_map/reduce_scatter | solution.py:169
  128.6 5.9 %copy-start.1 = (bf16[1024,8,512]{0,2,1:T(8,128)(2,1)S(1)}, bf16[1024,8,512]{0,2,1:T(8,128)(2,1)}, u32[]{:S(2)}) copy-start(bf16[1024,8,512]{0,2,1:T(8,128)(2,1)} %copy.37) | copy-start | bytes 25165828
  149.2 6.1 %slice-start.4 = ((s8[5242880]{0:T(1024)(128)(4,1)}), s8[1048576]{0:T(1024)(128)(4,1)S(1)}, s32[]{:S(2)}) async-start(s8[5242880]{0:T(1024)(128)(4,1)} %bitcast.79), calls=%async_computation.10 | async-start | bytes 2097152
  149.5 5.7 %slice-start.5 = ((s8[5242880]{0:T(1024)(128)(4,1)}), s8[4194304]{0:T(1024)(128)(4,1)S(1)}, s32[]{:S(2)}) async-start(s8[5242880]{0:T(1024)(128)(4,1)} %bitcast.79), calls=%async_computation.11 | async-start | bytes 8388608
  149.5 11.8 %slice-start.2 = ((s8[8388608]{0:T(1024)(128)(4,1)}), s8[4194304]{0:T(1024)(128)(4,1)S(1)}, s32[]{:S(2)}) async-start(s8[8388608]{0:T(1024)(128)(4,1)} %bitcast.74), calls=%async_computation.8 | async-start | bytes 8388608
  154.7 11.8 %slice-start = ((s8[8388608]{0:T(1024)(128)(4,1)}), s8[4194304]{0:T(1024)(128)(4,1)S(1)}, s32[]{:S(2)}) async-start(s8[8388608]{0:T(1024)(128)(4,1)} %bitcast.71), calls=%async_computation.6 | async-start | bytes 8388608
  155.2 6.1 %slice-start.3 = ((s8[8388608]{0:T(1024)(128)(4,1)}), s8[4194304]{0:T(1024)(128)(4,1)S(1)}, s32[]{:S(2)}) async-start(s8[8388608]{0:T(1024)(128)(4,1)} %bitcast.74), calls=%async_computation.9 | async-start | bytes 8388608
  155.2 11.2 %slice-start.1 = ((s8[8388608]{0:T(1024)(128)(4,1)}), s8[4194304]{0:T(1024)(128)(4,1)S(1)}, s32[]{:S(2)}) async-start(s8[8388608]{0:T(1024)(128)(4,1)} %bitcast.71), calls=%async_computation.7 | async-start | bytes 8388608
  161.4 9.4 %copy-start.4 = (bf16[1024,256]{0,1:T(8,128)(2,1)}, bf16[1024,256]{0,1:T(8,128)(2,1)S(1)}, u32[]{:S(2)}) copy-start(bf16[1024,256]{0,1:T(8,128)(2,1)S(1)} %fusion.11) | copy-start | bytes 1572868
  161.4 5.1 %copy-start.3 = (bf16[256,4096]{1,0:T(8,128)(2,1)S(1)}, bf16[256,4096]{1,0:T(8,128)(2,1)}, u32[]{:S(2)}) copy-start(bf16[256,4096]{1,0:T(8,128)(2,1)} %copy.46) | copy-start | bytes 6291460
  163.4 7.4 %copy-start.6 = (bf16[1024,64]{0,1:T(8,128)(2,1)}, bf16[1024,64]{0,1:T(8,128)(2,1)S(1)}, u32[]{:S(2)}) copy-start(bf16[1024,64]{0,1:T(8,128)(2,1)S(1)} %convolution_convert_fusion) | copy-start | bytes 393220
  163.4 6.4 %collective-permute-start = (bf16[128,384]{0,1:T(8,128)(2,1)S(1)}, bf16[128,384]{0,1:T(8,128)(2,1)S(1)}, u32[]{:S(2)}, u32[]{:S(2)}) collective-permute-start(bf16[128,384]{0,1:T(8,128)(2,1)S(1)} %get-tuple-element.7), channel_id=1, source_target_pairs={{0,8},{8,16},{16,24},{24,32},{32,40},{40,48},{48,56},{56,64},{64,7... | collective-permute-start | bytes 294920 | tf_op jit(solution)/shard_map/ppermute | solution.py:32
  165.0 5.8 %collective-permute-start.1 = (bf16[128,384]{0,1:T(8,128)(2,1)S(1)}, bf16[128,384]{0,1:T(8,128)(2,1)S(1)}, u32[]{:S(2)}, u32[]{:S(2)}) collective-permute-start(bf16[128,384]{0,1:T(8,128)(2,1)S(1)} %get-tuple-element.8), channel_id=1, source_target_pairs={{8,0},{16,8},{24,16},{32,24},{40,32},{48,40},{56,48},{64,56},{72,6... | collective-permute-start | bytes 294920 | tf_op jit(solution)/shard_map/ppermute | solution.py:35
  169.8 1.3 copy-start.8
  170.8 0.6 copy-start.10
  173.4 5.2 %copy-start.15 = (f32[4]{0:T(128)S(1)}, f32[4]{0:T(128)}, u32[]{:S(2)}) copy-start(f32[4]{0:T(128)} %param.19) | copy-start | bytes 52
  178.6 7.0 %copy-start.2 = (f32[1,4,1024,1280]{2,3,1,0:T(8,128)}, f32[1,4,1024,1280]{2,3,1,0:T(8,128)S(1)}, u32[]{:S(2)}) copy-start(f32[1,4,1024,1280]{2,3,1,0:T(8,128)S(1)} %get-tuple-element.20) | copy-start | bytes 62914564
  185.6 1.2 copy-start.5
  185.6 1.2 copy-start.16
  185.6 1.2 copy-start.17
  185.6 1.2 copy-start.18
  185.7 1.2 copy-start.19
  185.7 1.2 copy-start.20
  186.9 10.7 %copy-start.7 = (bf16[1024,64]{0,1:T(8,128)(2,1)S(1)}, bf16[1024,64]{0,1:T(8,128)(2,1)}, u32[]{:S(2)}) copy-start(bf16[1024,64]{0,1:T(8,128)(2,1)} %copy-done.6) | copy-start | bytes 393220
  186.9 10.7 %copy-start.9 = (bf16[128,384]{0,1:T(8,128)(2,1)S(1)}, bf16[128,384]{0,1:T(8,128)(2,1)}, u32[]{:S(2)}) copy-start(bf16[128,384]{0,1:T(8,128)(2,1)} %copy-done.8) | copy-start | bytes 294916
  186.9 10.7 %copy-start.11 = (bf16[128,384]{0,1:T(8,128)(2,1)S(1)}, bf16[128,384]{0,1:T(8,128)(2,1)}, u32[]{:S(2)}) copy-start(bf16[128,384]{0,1:T(8,128)(2,1)} %copy-done.10) | copy-start | bytes 294916
Sparse Core Ops, SparseCore 0:
  10.0 85.5 all-gather.3
  97.4 36.9 all-gather.5
  136.2 40.9 all-gather.7
  219.1 59.0 reduce-scatter.1
